TPU v7x, 32 devices: a whole 2x2x4 slice. The times are simulated.
32 devices in a mesh: kv: 8 (over z, y), tp: 4 (over x, core).
Axes of the slice: x: 2, y: 2, z: 4, core: 2. Of those that a mesh axis runs over, the one named last changes fastest.
Arguments:
- tokens: bfloat16 [16, 4096], P(None, ('kv', 'tp')), may hold values from -8 to 8
- gate_weights: bfloat16 [2, 4096, 11264], P(None, None, ('kv', 'tp')), may hold values from -0.09375 to 0.09375
- up_weights: bfloat16 [2, 4096, 11264], P(None, None, ('kv', 'tp')), may hold values from -0.09375 to 0.09375
- down_weights: bfloat16 [2, 11264, 4096], P(None, ('kv', 'tp')), may hold values from -0.4375 to 0.4375
- norm_gain: bfloat16 [3, 4096], P(None, ('kv', 'tp')), may hold values from 0.25 to 4.5
- norm_bias: bfloat16 [3, 4096], P(None, ('kv', 'tp')), may hold values from -3 to 3
- query_weight: bfloat16 [4096, 4096], P('kv', 'tp'), may hold values from -0.09375 to 0.09375
- forget_weight: bfloat16 [4096, 4096], P('kv', 'tp'), may hold values from -0.09375 to 0.09375
- input_weight: bfloat16 [4096, 4096], P('kv', 'tp'), may hold values from -0.09375 to 0.09375
- outgate_weight: bfloat16 [4096, 4096], P('kv', 'tp'), may hold values from -0.09375 to 0.09375
- lower_bound: float32 [4096], P('tp'), may hold values from 0.05 to 0.9
- head_gain: float32 [4096], P('tp'), may hold values from 0.1 to 1.9
- out_weight: bfloat16 [4096, 4096], P('tp'), may hold values from -0.25 to 0.25
- state: float32 [16, 32, 128, 128], P('kv', 'tp'), may hold values from -3 to 3
Outputs:
- mixed: bfloat16 [16, 4096], P(None, ('kv', 'tp'))
- new_state: float32 [16, 32, 128, 128], P('kv', 'tp')
All inputs are finite; a program needn't handle non-finite values.
Results may differ from a plain program's by a relative error of at most 0.022.
Values may be sent and summed in bfloat16 or wider, within the bound.
A program may use at most 64 MiB of HBM per device.

v0:
```python
import jax
import jax.numpy as jnp
from jax import lax
from jax.sharding import PartitionSpec as P

HEAD = 128
residual_scale = 8.0**0.25
norm_eps = 1e-05
head_eps = 1e-06


def whole_norm(stream, gain_row, bias_row):
    row_mean = jnp.mean(stream, axis=-1, keepdims=True)
    centred = stream - row_mean
    spread = jnp.mean(centred * centred, axis=-1, keepdims=True)
    return centred * lax.rsqrt(spread + norm_eps) * gain_row.astype(jnp.float32) + bias_row.astype(
        jnp.float32
    )


def ffn_partial(whole_rows, gate_w, up_w, down_w):
    gate_proj = jnp.dot(whole_rows, gate_w, preferred_element_type=jnp.float32)
    up_proj = jnp.dot(whole_rows, up_w, preferred_element_type=jnp.float32)
    hidden = (jax.nn.silu(gate_proj) * up_proj).astype(jnp.bfloat16)
    return jnp.dot(hidden, down_w, preferred_element_type=jnp.float32)


def local(
    tokens,
    gate_weights,
    up_weights,
    down_weights,
    norm_gain,
    norm_bias,
    query_weight,
    forget_weight,
    input_weight,
    outgate_weight,
    lower_bound,
    head_gain,
    out_weight,
    state,
):
    own_cols = tokens.shape[1]
    col_offset = lax.axis_index(("kv", "tp")) * own_cols
    whole_tokens, whole_gain, whole_bias = (
        lax.all_gather(tokens, ("kv", "tp"), axis=1, tiled=True),
        lax.all_gather(norm_gain, ("kv", "tp"), axis=1, tiled=True),
        lax.all_gather(norm_bias, ("kv", "tp"), axis=1, tiled=True),
    )

    def finish(partial_value, residual_whole, index, want_whole):
        total = lax.psum(partial_value, ("kv", "tp"))
        stream = residual_scale * residual_whole + 0.5 * total
        normed = whole_norm(stream, whole_gain[index], whole_bias[index]).astype(jnp.bfloat16)
        if want_whole:
            return normed
        return lax.dynamic_slice_in_dim(normed, col_offset, own_cols, 1)

    partial_one = ffn_partial(whole_tokens, gate_weights[0], up_weights[0], down_weights[0])
    normed_one = finish(partial_one, whole_tokens.astype(jnp.float32), 0, True)
    seq_count = state.shape[0]
    head_count = state.shape[1]
    head_cols = query_weight.shape[1]
    weight_rows = query_weight.shape[0]
    seq_offset = lax.axis_index("kv") * seq_count
    block_rows = lax.dynamic_slice_in_dim(
        normed_one, lax.axis_index("kv") * weight_rows, weight_rows, 1
    )
    weights = (query_weight, forget_weight, input_weight, outgate_weight)
    projected = lax.psum_scatter(
        jnp.concatenate(
            [jnp.dot(block_rows, weight, preferred_element_type=jnp.float32) for weight in weights],
            axis=1,
        ).astype(jnp.bfloat16),
        "kv",
        scatter_dimension=0,
        tiled=True,
    )
    query_pre = projected[:, :head_cols].astype(jnp.float32).reshape(seq_count, head_count, HEAD)
    forget_pre = (
        projected[:, head_cols : 2 * head_cols]
        .astype(jnp.float32)
        .reshape(seq_count, head_count, HEAD)
    )
    input_pre = (
        projected[:, 2 * head_cols : 3 * head_cols]
        .astype(jnp.float32)
        .reshape(seq_count, head_count, HEAD)
    )
    outgate_pre = projected[:, 3 * head_cols :].astype(jnp.float32)
    low_bound = lower_bound.reshape(head_count, HEAD)
    forget = low_bound + (1.0 - low_bound) * jax.nn.sigmoid(forget_pre)
    key_part = (1.0 - low_bound) * jax.nn.sigmoid(-forget_pre)
    updated = forget[..., None] * state + key_part[..., None] * input_pre[:, :, None, :]
    readout = jnp.einsum(
        "shd,shde->she", jax.nn.silu(query_pre), updated, precision=lax.Precision.HIGHEST
    )
    readout = readout * lax.rsqrt(jnp.mean(readout * readout, axis=-1, keepdims=True) + head_eps)
    gated_out = (
        readout.reshape(seq_count, head_cols) * head_gain * jax.nn.silu(outgate_pre)
    ).astype(jnp.bfloat16)
    mixer_part = jnp.dot(gated_out, out_weight, preferred_element_type=jnp.float32)
    head_sum = lax.psum_scatter(
        mixer_part.astype(jnp.bfloat16), "tp", scatter_dimension=1, tiled=True
    ).astype(jnp.float32)
    piece_cols = head_sum.shape[1]
    own_normed = lax.dynamic_slice_in_dim(normed_one, seq_offset, seq_count, 0)
    own_normed = lax.dynamic_slice_in_dim(
        own_normed, lax.axis_index("tp") * piece_cols, piece_cols, 1
    )
    stream_own = (residual_scale * own_normed.astype(jnp.float32) + head_sum).astype(jnp.bfloat16)
    seq_rows = lax.all_gather(stream_own, "tp", axis=1, tiled=True)
    stream_two = lax.all_gather(seq_rows, "kv", axis=0, tiled=True)
    normed_two = whole_norm(stream_two.astype(jnp.float32), whole_gain[1], whole_bias[1]).astype(
        jnp.bfloat16
    )
    partial_two = ffn_partial(normed_two, gate_weights[1], up_weights[1], down_weights[1])
    mixed = finish(partial_two, normed_two.astype(jnp.float32), 2, False)
    return (mixed, updated)


def solution(mesh):
    return jax.shard_map(
        local,
        mesh=mesh,
        in_specs=(
            P(None, ("kv", "tp")),
            P(None, None, ("kv", "tp")),
            P(None, None, ("kv", "tp")),
            P(None, ("kv", "tp"), None),
            P(None, ("kv", "tp")),
            P(None, ("kv", "tp")),
            P("kv", "tp"),
            P("kv", "tp"),
            P("kv", "tp"),
            P("kv", "tp"),
            P("tp"),
            P("tp"),
            P("tp", None),
            P("kv", "tp", None, None),
        ),
        out_specs=(P(None, ("kv", "tp")), P("kv", "tp", None, None)),
        check_vma=False,
    )
```

profile of v0, /device:TPU:0, one launch (start us, length us, event | category | flops | bytes accessed | tf_op | source)
XLA Modules:
  0.0 475.1 jit_solution(1916518418078540519)
XLA Ops:
  7.3 44.0 %all_gather.15 = bf16[16,4096]{1,0:T(8,128)(2,1)S(1)} all-gather(bf16[16,128]{1,0:T(8,128)(2,1)} %param.14), channel_id=1, replica_groups=mesh['kv'=8,'tp'=4] {'kv','tp'}, dimensions={1}, use_global_device_ids=true | all-gather | bytes 135168 | tf_op jit(solution)/shard_map/all_gather | solution.py:47
  51.2 2.7 fusion.10
  54.0 5.5 %fusion.6 = f32[16,4096]{1,0:T(8,128)} fusion(bf16[2,352,4096]{2,1,0:T(8,128)(2,1)} %param.17, bf16[16,4096]{1,0:T(8,128)(2,1)S(1)} %all_gather.15, bf16[2,4096,352]{1,2,0:T(8,128)(2,1)} %param.16, f32[16,352]{1,0:T(8,128)S(1)} %fusion.10), kind=kOutput, calls=%fused_computation.7 | convolution fusion | flops 92308480 | bytes 6182912 | tf_op jit(solution)/shard_map/dot_general | solution.py:25
  59.6 36.7 %all_gather.16 = bf16[3,4096]{1,0:T(4,128)(2,1)S(1)} all-gather(bf16[3,128]{1,0:T(4,128)(2,1)S(1)} %copy-done.6), channel_id=1, replica_groups=mesh['kv'=8,'tp'=4] {'kv','tp'}, dimensions={1}, use_global_device_ids=true | all-gather | bytes 25344 | tf_op jit(solution)/shard_map/all_gather | solution.py:48
  96.3 38.1 %all_gather.17 = bf16[3,4096]{1,0:T(4,128)(2,1)S(1)} all-gather(bf16[3,128]{1,0:T(4,128)(2,1)S(1)} %copy-done.7), channel_id=1, replica_groups=mesh['kv'=8,'tp'=4] {'kv','tp'}, dimensions={1}, use_global_device_ids=true | all-gather | bytes 25344 | tf_op jit(solution)/shard_map/all_gather | solution.py:49
  135.7 46.7 %all-reduce.5.cloned.1.call-done = f32[16,4096]{1,0:T(8,128)} async-done(((f32[16,4096]{1,0:T(8,128)}), f32[16,4096]{1,0:T(8,128)}) %all-reduce.5.cloned.1.call-update) | async-done | bytes 262160 | tf_op jit(solution)/shard_map/psum | solution.py:53
  182.4 1.1 fusion.36
  183.5 1.2 multiply_reduce_fusion.2
  184.7 1.1 add_convert_fusion.1
  186.5 1.5 convolution_convert_fusion.4
  188.8 69.5 %all-reduce.9.cloned.1.call-done = bf16[16,4096]{1,0:T(8,128)(2,1)} async-done(((bf16[16,4096]{1,0:T(8,128)(2,1)}), bf16[16,4096]{1,0:T(8,128)(2,1)}) %all-reduce.9.cloned.1.call-update) | async-done | bytes 131088
  260.0 1.8 multiply_add_fusion
  261.8 1.0 fusion.83
  263.0 4.7 convolution_convert_fusion
  267.6 1.4 copy.18
  269.2 24.0 %reduce-scatter.4.cloned.1.call-done = bf16[1024,2]{1,0:T(8,128)(2,1)} async-done(((bf16[4096,2]{1,0:T(8,128)(2,1)}), bf16[1024,2]{1,0:T(8,128)(2,1)}) %reduce-scatter.4.cloned.1.call-update) | async-done | bytes 4112
  293.1 1.1 copy.19
  294.3 5.2 %all_gather.18 = bf16[2,4096]{1,0:T(2,128)(2,1)S(1)} all-gather(bf16[2,1024]{1,0:T(2,128)(2,1)S(1)} %add_convert_fusion.2), channel_id=1, replica_groups=mesh['kv'=8,'tp'=4] {'tp'}, dimensions={1}, use_global_device_ids=true | all-gather | bytes 20480 | tf_op jit(solution)/shard_map/all_gather | solution.py:113
  299.5 30.6 %all-gather = bf16[8,2,4096]{2,1,0:T(2,128)(2,1)S(1)} all-gather(bf16[1,2,4096]{2,1,0:T(2,128)(2,1)S(1)} %bitcast.107), channel_id=1, replica_groups=mesh['kv'=8,'tp'=4] {'kv'}, dimensions={0}, use_global_device_ids=true | all-gather | bytes 147456 | tf_op jit(solution)/shard_map/all_gather | solution.py:114
  330.6 2.7 fusion.4
  333.3 5.4 %fusion = f32[16,4096]{1,0:T(8,128)} fusion(bf16[2,352,4096]{2,1,0:T(8,128)(2,1)} %param.17, bf16[2,4096,352]{1,2,0:T(8,128)(2,1)} %param.16, f32[16,352]{1,0:T(8,128)S(1)} %fusion.4, f32[16,4096]{1,0:T(8,128)S(1)} %reshape.110, f32[4096]{0:T(1024)S(1)} %bitcast.101, f32[4096]{0:T(1024)S(1)} %bitcast.97, f32[16]{0:T(128)S(1)} %add_rsqrt_fusion.2, ...), kind=kOutput, calls=%fused_computation.1 | convolution fusion | flops 92636160 | bytes 6346880 | tf_op jit(solution)/shard_map/dot_general | solution.py:25
  338.9 126.6 %all-reduce.7.cloned.1.call-done = f32[16,4096]{1,0:T(8,128)} async-done(((f32[16,4096]{1,0:T(8,128)}), f32[16,4096]{1,0:T(8,128)}) %all-reduce.7.cloned.1.call-update) | async-done | bytes 262160 | tf_op jit(solution)/shard_map/psum | solution.py:53
  465.5 1.2 fusion.35
  466.7 1.2 multiply_reduce_fusion
  (56 shorter events, 5.7 us)
Async XLA Ops:
  7.2 178.6 %copy-start = (bf16[512,1024]{1,0:T(8,128)(2,1)S(1)}, bf16[512,1024]{1,0:T(8,128)(2,1)}, u32[]{:S(2)}) copy-start(bf16[512,1024]{1,0:T(8,128)(2,1)} %param.21) | copy-start | bytes 3145732
  7.2 127.3 %copy-start.8 = (u32[32]{0:T(128)S(1)}, u32[32]{0:T(128)}, u32[]{:S(2)}) copy-start(u32[32]{0:T(128)} %constant.72) | copy-start | bytes 388
  7.2 52.4 %copy-start.6 = (bf16[3,128]{1,0:T(4,128)(2,1)S(1)}, bf16[3,128]{1,0:T(4,128)(2,1)}, u32[]{:S(2)}) copy-start(bf16[3,128]{1,0:T(4,128)(2,1)} %param.18) | copy-start | bytes 2308
  7.2 89.1 %copy-start.7 = (bf16[3,128]{1,0:T(4,128)(2,1)S(1)}, bf16[3,128]{1,0:T(4,128)(2,1)}, u32[]{:S(2)}) copy-start(bf16[3,128]{1,0:T(4,128)(2,1)} %param.19) | copy-start | bytes 2308
  7.2 175.2 %all-reduce.5.cloned.1.call-start = ((), (), s32[]{:S(2)}) async-start(), calls=%async_computation.1 | async-start | bytes 524288 | tf_op jit(solution)/shard_map/psum | solution.py:53
  51.2 134.8 %copy-start.2 = (bf16[512,1024]{1,0:T(8,128)(2,1)S(1)}, bf16[512,1024]{1,0:T(8,128)(2,1)}, u32[]{:S(2)}) copy-start(bf16[512,1024]{1,0:T(8,128)(2,1)} %param.22) | copy-start | bytes 3145732
  54.0 132.3 %copy-start.3 = (bf16[512,1024]{1,0:T(8,128)(2,1)S(1)}, bf16[512,1024]{1,0:T(8,128)(2,1)}, u32[]{:S(2)}) copy-start(bf16[512,1024]{1,0:T(8,128)(2,1)} %param.23) | copy-start | bytes 3145732
  54.0 134.8 %copy-start.5 = (f32[1024]{0:T(1024)S(1)}, f32[1024]{0:T(1024)}, u32[]{:S(2)}) copy-start(f32[1024]{0:T(1024)} %param.24) | copy-start | bytes 12292
  59.5 203.5 %copy-start.4 = (f32[1024]{0:T(1024)S(1)}, f32[1024]{0:T(1024)}, u32[]{:S(2)}) copy-start(f32[1024]{0:T(1024)} %param.25) | copy-start | bytes 12292
  59.5 198.8 %all-reduce.9.cloned.1.call-start = ((), (), s32[]{:S(2)}) async-start(), calls=%async_computation.4 | async-start | bytes 262144
  188.7 104.4 %reduce-scatter.4.cloned.1.call-start = ((), (), s32[]{:S(2)}) async-start(), calls=%async_computation.3 | async-start | bytes 1310720
  261.8 5.8 %copy-start.1 = (f32[2,8,128,128]{3,2,1,0:T(8,128)}, f32[2,8,128,128]{3,2,1,0:T(8,128)S(1)}, u32[]{:S(2)}) copy-start(f32[2,8,128,128]{3,2,1,0:T(8,128)S(1)} %multiply_add_fusion) | copy-start | bytes 3145732
  269.1 196.4 %all-reduce.7.cloned.1.call-start = ((), (), s32[]{:S(2)}) async-start(), calls=%async_computation.2 | async-start | bytes 524288 | tf_op jit(solution)/shard_map/psum | solution.py:53
Sparse Core Ops, SparseCore 0:
  59.6 122.7 all-reduce.4
  188.8 69.4 all-reduce.8
  269.2 23.8 reduce-scatter.3
  338.9 126.5 all-reduce.6
where the time goes:
time: 476 us; the launch traced here: 475 us
  waiting for transfers between devices  267 us (56%)
  blocking collectives  155 us (33%)
  matrix products  24.2 us (5%)
  between operations  14.6 us (3%)
  other arithmetic  11.4 us (2%)
    psum x2, waiting for transfers between devices, finish(): total = lax.psum(partial_value, ('kv', 'tp'))  173 us
    unnamed x6, waiting for transfers between devices  93.6 us
    all_gather x1, blocking collectives, local(): lax.all_gather(tokens, ('kv', 'tp'), axis=1, tiled=True)  44 us
    all_gather x1, blocking collectives, local(): lax.all_gather(norm_bias, ('kv', 'tp'), axis=1, tiled=True)  38.1 us
    all_gather x1, blocking collectives, local(): lax.all_gather(norm_gain, ('kv', 'tp'), axis=1, tiled=True)  36.7 us
    all_gather x1, blocking collectives, local(): stream_two = lax.all_gather(seq_rows, 'kv', axis=0, tiled=True)  30.6 us
    dot_general x2, matrix products, ffn_partial(): return jnp.dot(hidden, down_w, preferred_element_type=jnp.float32)  10.9 us
  transfers between devices with their start and end apart: 4, of which 4 were waited for; matrix products, arithmetic and copies ran while one was open for 0% of the time, Pallas kernels for 0%

commit v1 on v0

--- a/solution.py
+++ b/solution.py
@@ -50,7 +50,8 @@
     )
 
     def finish(partial_value, residual_whole, index, want_whole):
-        total = lax.psum(partial_value, ("kv", "tp"))
+        blocks = lax.all_gather(partial_value, ("kv", "tp"))
+        total = jnp.sum(blocks, axis=0)
         stream = residual_scale * residual_whole + 0.5 * total
         normed = whole_norm(stream, whole_gain[index], whole_bias[index]).astype(jnp.bfloat16)
         if want_whole:

time: 476 us -> 384 us (0.81)
  waiting for transfers between devices: 267 us -> 166 us
  other arithmetic: 11.4 us -> 18.4 us
    psum x2 -> x0, waiting for transfers between devices: 173 us -> none  [finish(): total = lax.psum(partial_value, ('kv', 'tp'))]
    all_gather x0 -> x2, waiting for transfers between devices: none -> 75.6 us  [finish(): blocks = lax.all_gather(partial_value, ('kv', 'tp'))]
    reduce_sum x0 -> x2, other arithmetic: none -> 7.66 us  [finish(): total = jnp.sum(blocks, axis=0)]
  transfers between devices with their start and end apart: 4 -> 4, of which waited for: 4 -> 3; matrix products, arithmetic and copies ran while one was open for 0% -> 1% of each run, Pallas kernels for 0% -> 0%
where the time goes in v1:
time: 384 us; the launch traced here: 383 us
  waiting for transfers between devices  166 us (43%)
  blocking collectives  155 us (40%)
  matrix products  24 us (6%)
  other arithmetic  18.4 us (5%)
  between operations  14.6 us (4%)
  local copies, waits for them, and re-layouts  4.75 us (1%)
    unnamed x6, waiting for transfers between devices  90.1 us
    all_gather x2, waiting for transfers between devices, finish(): blocks = lax.all_gather(partial_value, ('kv', 'tp'))  75.6 us
    all_gather x1, blocking collectives, local(): lax.all_gather(tokens, ('kv', 'tp'), axis=1, tiled=True)  44 us
    all_gather x1, blocking collectives, local(): lax.all_gather(norm_bias, ('kv', 'tp'), axis=1, tiled=True)  38.8 us
    all_gather x1, blocking collectives, local(): lax.all_gather(norm_gain, ('kv', 'tp'), axis=1, tiled=True)  36.9 us
    all_gather x1, blocking collectives, local(): stream_two = lax.all_gather(seq_rows, 'kv', axis=0, tiled=True)  30.5 us
    dot_general x2, matrix products, ffn_partial(): return jnp.dot(hidden, down_w, preferred_element_type=jnp.float32)  10.8 us
  transfers between devices with their start and end apart: 4, of which 3 were waited for; matrix products, arithmetic and copies ran while one was open for 1% of the time, Pallas kernels for 0%

profile of v1, /device:TPU:0, one launch (start us, length us, event | category | flops | bytes accessed | tf_op | source)
XLA Modules:
  0.0 383.0 jit_solution(1239892328921686966)
XLA Ops:
  7.3 44.0 %all_gather.27 = bf16[16,4096]{1,0:T(8,128)(2,1)S(1)} all-gather(bf16[16,128]{1,0:T(8,128)(2,1)} %param.14), channel_id=1, replica_groups=mesh['kv'=8,'tp'=4] {'kv','tp'}, dimensions={1}, use_global_device_ids=true | all-gather | bytes 135168 | tf_op jit(solution)/shard_map/all_gather | solution.py:47
  51.2 2.7 fusion.10
  53.9 5.4 %fusion.6 = f32[16,4096]{1,0:T(8,128)} fusion(bf16[2,352,4096]{2,1,0:T(8,128)(2,1)} %param.17, bf16[16,4096]{1,0:T(8,128)(2,1)S(1)} %all_gather.27, bf16[2,4096,352]{1,2,0:T(8,128)(2,1)} %param.16, f32[16,352]{1,0:T(8,128)S(1)} %fusion.10), kind=kOutput, calls=%fused_computation.7 | convolution fusion | flops 92308480 | bytes 6182912 | tf_op jit(solution)/shard_map/dot_general | solution.py:25
  60.7 36.9 %all_gather.30 = bf16[3,4096]{1,0:T(4,128)(2,1)S(1)} all-gather(bf16[3,128]{1,0:T(4,128)(2,1)S(1)} %copy-done.7), channel_id=1, replica_groups=mesh['kv'=8,'tp'=4] {'kv','tp'}, dimensions={1}, use_global_device_ids=true | all-gather | bytes 25344 | tf_op jit(solution)/shard_map/all_gather | solution.py:48
  97.5 38.8 %all_gather.31 = bf16[3,4096]{1,0:T(4,128)(2,1)S(1)} all-gather(bf16[3,128]{1,0:T(4,128)(2,1)S(1)} %copy-done.8), channel_id=1, replica_groups=mesh['kv'=8,'tp'=4] {'kv','tp'}, dimensions={1}, use_global_device_ids=true | all-gather | bytes 25344 | tf_op jit(solution)/shard_map/all_gather | solution.py:49
  137.6 3.9 %reduce_sum.81 = f32[16,4096]{1,0:T(8,128)S(1)} reduce(f32[32,16,4096]{2,1,0:T(8,128)} %bitcast.97, f32[]{:T(128)} %constant.50.clone.1), dimensions={0}, to_apply=%region_0.1 | reduce | flops 2031616 | bytes 8650756 | tf_op jit(solution)/shard_map/reduce_sum | solution.py:54
  141.9 0.9 add_convert_fusion.1
  143.5 1.5 convolution_convert_fusion.4
  146.5 66.0 %all-reduce.3.cloned.1.call-done = bf16[16,4096]{1,0:T(8,128)(2,1)} async-done(((bf16[16,4096]{1,0:T(8,128)(2,1)}), bf16[16,4096]{1,0:T(8,128)(2,1)}) %all-reduce.3.cloned.1.call-update) | async-done | bytes 131088
  212.5 0.8 convert_bitcast_fusion
  213.3 0.8 fusion.57
  214.8 1.8 multiply_add_fusion
  216.7 1.0 fusion.83
  217.8 4.7 %convolution_convert_fusion = bf16[2,4096]{1,0:T(2,128)(2,1)S(1)} fusion(bf16[1024,4096]{1,0:T(8,128)(2,1)} %param.26, f32[1,2,8,128]{3,2,1,0:T(8,128)S(1)} %multiply_bitcast_fusion, bf16[16,4096]{1,0:T(8,128)(2,1)} %all-reduce.3.cloned.1.call-done, u32[]{:T(128)S(6)} %multiply.43, u32[]{:T(128)S(6)} %convert.26, f32[1024]{0:T(1024)S(1)} %copy-done.6), kind=kOutput, calls=%fused_computation | convolution fusion | flops 16801792 | bytes 8421384 | tf_op jit(solution)/shard_map/dot_general | solution.py:104
  222.5 1.4 copy.18
  224.0 24.0 %reduce-scatter.4.cloned.1.call-done = bf16[1024,2]{1,0:T(8,128)(2,1)} async-done(((bf16[4096,2]{1,0:T(8,128)(2,1)}), bf16[1024,2]{1,0:T(8,128)(2,1)}) %reduce-scatter.4.cloned.1.call-update) | async-done | bytes 4112
  248.0 1.1 copy.19
  249.1 0.9 add_convert_fusion.2
  249.9 5.2 %all_gather.32 = bf16[2,4096]{1,0:T(2,128)(2,1)S(1)} all-gather(bf16[2,1024]{1,0:T(2,128)(2,1)S(1)} %add_convert_fusion.2), channel_id=1, replica_groups=mesh['kv'=8,'tp'=4] {'tp'}, dimensions={1}, use_global_device_ids=true | all-gather | bytes 20480 | tf_op jit(solution)/shard_map/all_gather | solution.py:114
  255.1 30.5 %all-gather.2 = bf16[8,2,4096]{2,1,0:T(2,128)(2,1)S(1)} all-gather(bf16[1,2,4096]{2,1,0:T(2,128)(2,1)S(1)} %bitcast.111), channel_id=1, replica_groups=mesh['kv'=8,'tp'=4] {'kv'}, dimensions={0}, use_global_device_ids=true | all-gather | bytes 147456 | tf_op jit(solution)/shard_map/all_gather | solution.py:115
  286.2 2.7 fusion.4
  288.9 5.4 %fusion = f32[16,4096]{1,0:T(8,128)} fusion(bf16[2,352,4096]{2,1,0:T(8,128)(2,1)} %param.17, bf16[2,4096,352]{1,2,0:T(8,128)(2,1)} %param.16, f32[16,352]{1,0:T(8,128)S(1)} %fusion.4, f32[16,4096]{1,0:T(8,128)S(1)} %reshape.112, f32[4096]{0:T(1024)S(1)} %bitcast.105, f32[4096]{0:T(1024)S(1)} %bitcast.101, f32[16]{0:T(128)S(1)} %add_rsqrt_fusion.2, ...), kind=kOutput, calls=%fused_computation.1 | convolution fusion | flops 92636160 | bytes 6346880 | tf_op jit(solution)/shard_map/dot_general | solution.py:25
  295.8 75.6 %all-gather.8.cloned.1.call-done = f32[512,4096]{1,0:T(8,128)} async-done(((f32[16,4096]{1,0:T(8,128)}), f32[512,4096]{1,0:T(8,128)}) %all-gather.8.cloned.1.call-update) | async-done | bytes 8388624 | tf_op jit(solution)/shard_map/all_gather | solution.py:53
  371.5 3.8 reduce_sum.87
  (60 shorter events, 8.8 us)
Async XLA Ops:
  7.2 135.6 %copy-start = (bf16[512,1024]{1,0:T(8,128)(2,1)S(1)}, bf16[512,1024]{1,0:T(8,128)(2,1)}, u32[]{:S(2)}) copy-start(bf16[512,1024]{1,0:T(8,128)(2,1)} %param.21) | copy-start | bytes 3145732
  7.2 52.2 %copy-start.9 = (u32[32]{0:T(128)S(1)}, u32[32]{0:T(128)}, u32[]{:S(2)}) copy-start(u32[32]{0:T(128)} %constant.72) | copy-start | bytes 388
  7.2 53.5 %copy-start.7 = (bf16[3,128]{1,0:T(4,128)(2,1)S(1)}, bf16[3,128]{1,0:T(4,128)(2,1)}, u32[]{:S(2)}) copy-start(bf16[3,128]{1,0:T(4,128)(2,1)} %param.18) | copy-start | bytes 2308
  7.2 90.3 %copy-start.8 = (bf16[3,128]{1,0:T(4,128)(2,1)S(1)}, bf16[3,128]{1,0:T(4,128)(2,1)}, u32[]{:S(2)}) copy-start(bf16[3,128]{1,0:T(4,128)(2,1)} %param.19) | copy-start | bytes 2308
  7.2 130.4 %all-gather.6.cloned.1.call-start = ((), (), s32[]{:S(2)}) async-start(), calls=%async_computation.1 | async-start | bytes 8650752 | tf_op jit(solution)/shard_map/all_gather | solution.py:53
  59.3 83.7 %copy-start.2 = (bf16[512,1024]{1,0:T(8,128)(2,1)S(1)}, bf16[512,1024]{1,0:T(8,128)(2,1)}, u32[]{:S(2)}) copy-start(bf16[512,1024]{1,0:T(8,128)(2,1)} %param.22) | copy-start | bytes 3145732
  59.3 153.1 %all-reduce.3.cloned.1.call-start = ((), (), s32[]{:S(2)}) async-start(), calls=%async_computation.4 | async-start | bytes 262144
  137.6 5.7 %copy-start.3 = (bf16[512,1024]{1,0:T(8,128)(2,1)S(1)}, bf16[512,1024]{1,0:T(8,128)(2,1)}, u32[]{:S(2)}) copy-start(bf16[512,1024]{1,0:T(8,128)(2,1)} %param.23) | copy-start | bytes 3145732
  142.7 0.8 copy-start.4
  142.8 75.1 %copy-start.6 = (f32[1024]{0:T(1024)S(1)}, f32[1024]{0:T(1024)}, u32[]{:S(2)}) copy-start(f32[1024]{0:T(1024)} %param.25) | copy-start | bytes 12292
  145.7 102.3 %reduce-scatter.4.cloned.1.call-start = ((), (), s32[]{:S(2)}) async-start(), calls=%async_computation.3 | async-start | bytes 1310720
  216.7 5.8 %copy-start.1 = (f32[2,8,128,128]{3,2,1,0:T(8,128)}, f32[2,8,128,128]{3,2,1,0:T(8,128)S(1)}, u32[]{:S(2)}) copy-start(f32[2,8,128,128]{3,2,1,0:T(8,128)S(1)} %multiply_add_fusion) | copy-start | bytes 3145732
  217.8 68.4 %copy-start.5 = (f32[1,4096]{1,0:T(1,128)S(1)}, f32[1,4096]{1,0:T(1,128)}, u32[]{:S(2)}) copy-start(f32[1,4096]{1,0:T(1,128)} %get-tuple-element.12) | copy-start | bytes 49156
  223.9 147.5 %all-gather.8.cloned.1.call-start = ((), (), s32[]{:S(2)}) async-start(), calls=%async_computation.2 | async-start | bytes 8650752 | tf_op jit(solution)/shard_map/all_gather | solution.py:53
Sparse Core Ops, SparseCore 0:
  59.5 73.3 all-gather.5
  145.8 66.5 all-reduce.2
  224.1 23.8 reduce-scatter.3
  294.4 76.9 all-gather.7
